TPU v7x, 32 devices: a whole 2x2x4 slice. The times are simulated.
32 devices in a mesh: sp: 8 (over z, x), dp: 4 (over y, core).
Axes of the slice: x: 2, y: 2, z: 4, core: 2. Of those that a mesh axis runs over, the one named last changes fastest.
Arguments:
- queries: bfloat16 [4, 1024, 16, 128], P('dp', 'sp'), may hold values from -3.5 to 2
- key_rows: bfloat16 [4, 1024, 16, 128], P('dp', 'sp'), may hold values from -4 to 5.3
- values: bfloat16 [4, 1024, 16, 128], P('dp', 'sp'), may hold values from -6 to 6
- residual: bfloat16 [4, 1024, 4096], P('dp', 'sp'), may hold values from -6 to 6
- out_weight: bfloat16 [2048, 4096], P(None, 'dp'), may hold values from -0.125 to 0.125
- mixer_gain: float32 [4096], replicated, may hold values from 0.1 to 1.9
- expert_gain: float32 [4096], replicated, may hold values from 0.1 to 1.9
- gate_weight: bfloat16 [32, 4096, 512], P(('sp', 'dp')), may hold values from -0.09375 to 0.09375
- up_weight: bfloat16 [32, 4096, 512], P(('sp', 'dp')), may hold values from -0.09375 to 0.09375
- expert_down_matrix: bfloat16 [32, 512, 4096], P(('sp', 'dp')), may hold values from -0.25 to 0.25
- routes: int32 [4, 1024, 2], P('dp', 'sp'), may hold values from 0 to 31, all different within a row; in each aligned block of 128 rows (0 to 127, 128 to 255, ..., all dimensions but the last counted through in order) at most 12 rows name the same one
- route_weight: float32 [4, 1024, 2], P('dp', 'sp'), may hold values from 0.1 to 1
- output_gain: float32 [4096], replicated, may hold values from 0.1 to 1.9
Outputs:
- output: bfloat16 [4, 1024, 4096], P('dp', 'sp')
Inputs may be any that keep to these rules, and one draw needn't show every extreme that they name: `routes`: each row names 2 different experts. Among the rows of one device no expert is named more than 12 times, and in every draw some device names some expert exactly 12 times.
All inputs are finite; a program needn't handle non-finite values.
Results may differ from a plain program's by a relative error of at most 0.009.
Values may be sent and summed in bfloat16 or wider, within the bound.
A program may use at most 192 MiB of HBM per device.

v0:
```python
import jax
import jax.numpy as jnp
from jax import lax
from jax.sharding import PartitionSpec as P

EPSILON = 1e-06


def normed_token_rows(matrix, gain):
    return matrix * lax.rsqrt(jnp.mean(matrix * matrix, axis=-1, keepdims=True) + EPSILON) * gain


def attend(query_rows, key_part, value_part):
    length = query_rows.shape[0]
    block_rows = min(512, length)
    score_scale = query_rows.shape[2] ** (-0.5)
    pieces = []
    for block_index in range(length // block_rows):
        row_start = block_index * block_rows
        row_stop = row_start + block_rows
        scores = (
            jnp.einsum(
                "qhd,khd->hqk",
                query_rows[row_start:row_stop],
                key_part[:row_stop],
                preferred_element_type=jnp.float32,
            )
            * score_scale
        )
        key_pos = lax.broadcasted_iota(jnp.int32, (1, block_rows, row_stop), 2)
        query_pos = lax.broadcasted_iota(jnp.int32, (1, block_rows, row_stop), 1) + row_start
        is_past = key_pos < query_pos
        log_keep = jnp.where(is_past, -jax.nn.softplus(scores), 0.0)
        suffix = lax.cumsum(log_keep, axis=2, reverse=True) - log_keep
        weights = jnp.where(is_past, jnp.exp(jax.nn.log_sigmoid(scores) + suffix), 0.0).astype(
            jnp.bfloat16
        )
        pieces.append(
            jnp.einsum(
                "hqk,khd->qhd", weights, value_part[:row_stop], preferred_element_type=jnp.float32
            ).astype(jnp.bfloat16)
        )
    return jnp.concatenate(pieces, axis=0)


def local(
    queries,
    key_rows,
    values,
    residual,
    out_weight,
    mixer_gain,
    expert_gain,
    gate_weight,
    up_weight,
    expert_down_matrix,
    routes,
    route_weight,
    output_gain,
):
    head_queries, head_keys, head_values = (
        lax.all_to_all(queries, "sp", split_axis=2, concat_axis=1, tiled=True),
        lax.all_to_all(key_rows, "sp", split_axis=2, concat_axis=1, tiled=True),
        lax.all_to_all(values, "sp", split_axis=2, concat_axis=1, tiled=True),
    )
    attended = attend(head_queries[0], head_keys[0], head_values[0])
    token_major = lax.all_to_all(attended[None], "sp", split_axis=1, concat_axis=2, tiled=True)
    local_rows = token_major.shape[1]
    flat_attn = token_major.reshape(local_rows, -1)
    projected = jnp.dot(
        flat_attn,
        lax.all_gather(out_weight, "dp", axis=1, tiled=True),
        preferred_element_type=jnp.float32,
    )
    stream = (residual[0].astype(jnp.float32) + normed_token_rows(projected, mixer_gain)).astype(
        jnp.bfloat16
    )
    expert_in = normed_token_rows(stream.astype(jnp.float32), expert_gain).astype(jnp.bfloat16)
    feature_count = expert_in.shape[1]
    experts = lax.axis_size("sp") * lax.axis_size("dp")
    top_count = routes.shape[2]
    capacity = max(2, 3 * local_rows // experts)
    picked_experts = routes[0].reshape(local_rows * top_count)
    onehot = (
        picked_experts[:, None]
        == lax.broadcasted_iota(jnp.int32, (local_rows * top_count, experts), 1)
    ).astype(jnp.int32)
    before = jnp.cumsum(onehot, axis=0) - onehot
    slot_rank = jnp.sum(before * onehot, axis=1)
    slot_index = slot_rank * experts + picked_experts
    source_row = lax.iota(jnp.int32, local_rows * top_count) // top_count
    slot_rows = (
        jnp.full((capacity * experts,), local_rows, jnp.int32).at[slot_index].set(source_row)
    )
    padded = jnp.concatenate([expert_in, jnp.zeros((1, feature_count), jnp.bfloat16)], axis=0)
    outgoing = jnp.take(padded, slot_rows, axis=0).reshape(capacity, experts, feature_count)
    arrived = lax.all_to_all(outgoing, ("sp", "dp"), split_axis=1, concat_axis=1, tiled=True)
    slot_count, sources, width_now = arrived.shape
    flat_rows = arrived.reshape(slot_count * sources, width_now)
    gate_out = jnp.dot(flat_rows, gate_weight[0], preferred_element_type=jnp.float32)
    upward = jnp.dot(flat_rows, up_weight[0], preferred_element_type=jnp.float32)
    hidden = (jax.nn.silu(gate_out) * upward).astype(jnp.bfloat16)
    result = jnp.dot(hidden, expert_down_matrix[0], preferred_element_type=jnp.float32).astype(
        jnp.bfloat16
    )
    returned = lax.all_to_all(
        result.reshape(slot_count, sources, width_now),
        ("sp", "dp"),
        split_axis=1,
        concat_axis=1,
        tiled=True,
    )
    gathered = jnp.take(returned.reshape(capacity * experts, feature_count), slot_index, axis=0)
    gathered = gathered.reshape(local_rows, top_count, feature_count)
    combined = jnp.sum(gathered.astype(jnp.float32) * route_weight[0][:, :, None], axis=1)
    output = (stream.astype(jnp.float32) + normed_token_rows(combined, output_gain)).astype(
        jnp.bfloat16
    )
    return output[None]


def solution(mesh):
    in_specs = (
        P("dp", "sp", None, None),
        P("dp", "sp", None, None),
        P("dp", "sp", None, None),
        P("dp", "sp", None),
        P(None, "dp"),
        P(),
        P(),
        P(("sp", "dp"), None, None),
        P(("sp", "dp"), None, None),
        P(("sp", "dp"), None, None),
        P("dp", "sp", None),
        P("dp", "sp", None),
        P(),
    )
    out_specs = P("dp", "sp", None)
    return jax.shard_map(local, mesh=mesh, in_specs=in_specs, out_specs=out_specs, check_vma=False)
```

profile of v0, /device:TPU:0, one launch (start us, length us, event | category | flops | bytes accessed | tf_op | source)
XLA Modules:
  0.0 405.7 jit_solution(7910260040351339867)
XLA Ops:
  6.6 0.7 all-gather.2.cloned.1.call-update
  7.3 0.3 copy-done.6
  7.6 0.9 copy.85
  8.5 7.3 %all-to-all-start = ((bf16[1,128,16,128]{3,1,0,2:T(8,128)(2,1)}), bf16[1,128,16,128]{3,1,0,2:T(8,128)(2,1)S(1)}, u32[]{:S(2)}, u32[]{:S(2)}) async-start(bf16[1,128,16,128]{3,1,0,2:T(8,128)(2,1)} %copy.85), calls=%async_computation | async-start | bytes 1048576 | tf_op jit(solution)/shard_map/all_to_all | solution.py:62
  15.8 0.1 copy.99
  15.9 0.1 eq.23
  16.0 0.1 eq.20
  16.2 0.9 copy.87
  17.1 0.9 copy.91
  18.1 12.2 %all-to-all-done = bf16[1,128,16,128]{3,1,0,2:T(8,128)(2,1)S(1)} async-done(((bf16[1,128,16,128]{3,1,0,2:T(8,128)(2,1)}), bf16[1,128,16,128]{3,1,0,2:T(8,128)(2,1)S(1)}, u32[]{:S(2)}, u32[]{:S(2)}) %all-to-all-start) | async-done | bytes 524320 | tf_op jit(solution)/shard_map/all_to_all | solution.py:62
  30.3 3.6 all-to-all-start.1
  33.9 0.6 reduce-window.26
  34.5 0.2 slice_reduce_fusion
  34.7 0.1 fusion.47
  34.9 0.4 iota_compare_fusion
  35.4 13.2 %all-to-all-done.1 = bf16[1,128,16,128]{3,1,0,2:T(8,128)(2,1)S(1)} async-done(((bf16[1,128,16,128]{3,1,0,2:T(8,128)(2,1)}), bf16[1,128,16,128]{3,1,0,2:T(8,128)(2,1)S(1)}, u32[]{:S(2)}, u32[]{:S(2)}) %all-to-all-start.1) | async-done | bytes 524320 | tf_op jit(solution)/shard_map/all_to_all | solution.py:63
  48.6 3.6 all-to-all-start.2
  52.3 5.2 %fusion.6 = (f32[2,512,1024]{2,1,0:T(8,128)S(1)}, f32[2,512,1024]{2,1,0:T(8,128)}) fusion(pred[512,1024]{1,0:T(8,128)(4,1)S(1)} %iota_compare_fusion, bf16[512,2,128]{2,0,1:T(8,128)(2,1)S(1)} %bitcast.129, bf16[1024,2,128]{2,0,1:T(8,128)(2,1)S(1)} %bitcast.124), kind=kOutput, calls=%fused_computation.14 | convolution fusion | flops 277872640 | bytes 9699328 | tf_op jit(solution)/shard_map/qhd,khd->hqk/dot_general | solution.py:22
  57.5 3.0 copy.113
  60.5 5.8 %copy.94 = f32[2,512,8,128]{1,2,3,0:T(8,128)} copy(f32[2,512,8,128]{3,2,1,0:T(8,128)} %bitcast.109) | data formatting | bytes 8388608 | tf_op jit(solution)/shard_map/reshape.3
  66.3 10.8 %fusion.57 = f32[2,512,8,128]{1,2,3,0:T(8,128)S(1)} fusion(f32[2,512,8,128]{1,2,3,0:T(8,128)} %copy.94), kind=kOutput, calls=%fused_computation.95 | output fusion | flops 133169152 | bytes 8388608 | tf_op jit(solution)/shard_map/reduce-window.2
  77.1 2.0 copy-done
  79.1 4.7 %broadcast_add_fusion = f32[2,512,8,128]{1,2,3,0:T(8,128)} fusion(f32[2,512,8,128]{1,2,3,0:T(8,128)} %copy-done, f32[2,512,8]{1,2,0:T(8,128)S(1)} %slice.67), kind=kLoop, calls=%fused_computation.44 | loop fusion | flops 1048576 | bytes 8421376 | tf_op jit(solution)/shard_map/reduce_window_sum | solution.py:34
  83.8 5.5 %copy.95 = f32[2,512,8,128]{3,2,1,0:T(8,128)} copy(f32[2,512,8,128]{1,2,3,0:T(8,128)} %broadcast_add_fusion) | data formatting | bytes 8388608 | tf_op jit(solution)/shard_map/reduce_window_sum | solution.py:34
  89.3 5.1 %reduce_window_sum.46 = f32[2,512,1024]{2,1,0:T(8,128)} reshape(f32[2,512,8,128]{3,2,1,0:T(8,128)} %copy.95) | data formatting | bytes 8388608 | tf_op jit(solution)/shard_map/reduce_window_sum | solution.py:34
  94.5 3.0 fusion.22
  97.6 9.6 %fusion.24 = f32[2,512,4,128]{1,2,3,0:T(4,128)S(1)} fusion(f32[2,512,4,128]{1,3,2,0:T(8,128)S(1)} %bitcast.116), kind=kOutput, calls=%fused_computation.40 | output fusion | flops 66584576 | bytes 4194304 | tf_op jit(solution)/shard_map/reduce-window
  107.3 0.8 broadcast_add_fusion.1
  108.1 0.6 copy.90
  108.7 0.9 copy-done.4
  109.6 3.2 fusion.20
  112.8 0.5 fusion.37
  113.4 7.2 %fusion.38 = bf16[512,2,128]{2,0,1:T(8,128)(2,1)S(1)} fusion(bf16[1024,2,128]{2,0,1:T(8,128)(2,1)S(1)} %bitcast.123, f32[2,512,1024]{2,1,0:T(8,128)S(1)} %copy-done.3, f32[2,512,1024]{2,1,0:T(8,128)S(1)} %copy-done.15, pred[512,1024]{1,0:T(8,128)(4,1)S(1)} %iota_compare_fusion), kind=kOutput, calls=%fused_computation.52 | convolution fusion | flops 290586624 | bytes 9699328 | tf_op jit(solution)/shard_map/hqk,khd->qhd/dot_general | solution.py:39
  120.6 1.3 copy.96
  122.0 6.0 %all-to-all-start.3 = ((bf16[1,1024,2,128]{3,2,0,1:T(2,128)(2,1)}), bf16[1,1024,2,128]{3,2,0,1:T(2,128)(2,1)S(1)}, u32[]{:S(2)}, u32[]{:S(2)}) async-start(bf16[1,1024,2,128]{3,2,0,1:T(2,128)(2,1)} %copy.96), calls=%async_computation.3 | async-start | bytes 1048576 | tf_op jit(solution)/shard_map/all_to_all | solution.py:67
  127.9 0.1 reshape_squeeze.3
  128.1 1.6 scatter_custom_fusion
  129.8 0.1 copy.105
  129.9 12.2 %all-to-all-done.3 = bf16[1,1024,2,128]{3,2,0,1:T(2,128)(2,1)S(1)} async-done(((bf16[1,1024,2,128]{3,2,0,1:T(2,128)(2,1)}), bf16[1,1024,2,128]{3,2,0,1:T(2,128)(2,1)S(1)}, u32[]{:S(2)}, u32[]{:S(2)}) %all-to-all-start.3) | async-done | bytes 524320 | tf_op jit(solution)/shard_map/all_to_all | solution.py:67
  142.2 0.3 copy.98
  142.5 8.3 %multiply_reduce_fusion.2 = (f32[128]{0:T(128)S(1)}, f32[128,4096]{1,0:T(8,128)S(1)}) fusion(bf16[128,2048]{0,1:T(8,128)(2,1)S(1)} %bitcast.115, bf16[2048,4096]{1,0:T(8,128)(2,1)} %all-gather.2.cloned.1.call-done), kind=kOutput, calls=%fused_computation.43 | convolution fusion | flops 2148532224 | bytes 19399168 | tf_op jit(solution)/shard_map/dot_general | solution.py:70
  150.8 0.7 fusion.12
  151.5 1.0 copy-done.1
  152.5 0.3 fusion.14
  152.8 0.1 concatenate.7
  152.9 4.0 gather_fusion
  157.0 5.7 %copy_select_fusion = bf16[12,32,4096]{2,0,1:T(8,128)(2,1)S(1)} fusion(bf16[12,32,4096]{2,1,0:T(8,128)(2,1)} %bitcast.110, pred[12,32]{0,1:T(8,128)(4,1)S(1)} %copy.105), kind=kLoop, calls=%fused_computation.20 | loop fusion | flops 1572864 | bytes 6291840 | tf_op jit(solution)/shard_map/jit(_take)/select_n | solution.py:96
  162.7 97.3 %all_to_all.70 = bf16[12,32,4096]{2,0,1:T(8,128)(2,1)S(1)} all-to-all(bf16[12,32,4096]{2,0,1:T(8,128)(2,1)S(1)} %copy_select_fusion), channel_id=1, replica_groups=mesh['sp'=8,'dp'=4] {'sp','dp'}, dimensions={1} | all-to-all | bytes 6291456 | tf_op jit(solution)/shard_map/all_to_all | solution.py:97
  260.0 1.7 copy.107
  261.7 0.5 copy-done.14
  262.2 2.7 fusion.10
  264.9 8.9 %convolution_convert_fusion = bf16[384,4096]{1,0:T(8,128)(2,1)} fusion(bf16[1,512,4096]{2,1,0:T(8,128)(2,1)} %param.22, bf16[384,4096]{1,0:T(8,128)(2,1)S(1)} %bitcast.113, bf16[1,4096,512]{2,1,0:T(8,128)(2,1)} %param.21, f32[384,512]{1,0:T(8,128)} %fusion.10), kind=kOutput, calls=%fused_computation.7 | convolution fusion | flops 3223977984 | bytes 15466496 | tf_op jit(solution)/shard_map/dot_general | solution.py:103
  273.8 5.6 %copy.108 = bf16[12,32,4096]{2,0,1:T(8,128)(2,1)} copy(bf16[12,32,4096]{2,1,0:T(8,128)(2,1)} %bitcast.114) | data formatting | bytes 6291456 | tf_op jit(solution)/shard_map/reshape | solution.py:107
  279.4 3.8 all-to-all-start.5
  283.2 0.1 mul.123
  283.5 0.1 copy.103
  283.6 0.1 copy.110
  283.7 93.7 %all-to-all-done.5 = bf16[12,32,4096]{2,0,1:T(8,128)(2,1)} async-done(((bf16[12,32,4096]{2,0,1:T(8,128)(2,1)}), bf16[12,32,4096]{2,0,1:T(8,128)(2,1)}, u32[]{:S(2)}, u32[]{:S(2)}) %all-to-all-start.5) | async-done | bytes 3145760 | tf_op jit(solution)/shard_map/all_to_all | solution.py:106
  377.5 3.9 copy.109
  381.4 3.2 gather_fusion.1
  384.6 3.4 gather.15
  388.0 8.7 %multiply_reduce_fusion = f32[128,4096]{1,0:T(8,128)S(1)} fusion(bf16[128,2,4096]{2,1,0:T(2,128)(2,1)S(1)} %gather.15, pred[128,2]{1,0:T(8,128)(4,1)S(1)} %copy.103, f32[128,2]{1,0:T(8,128)S(1)} %copy.110), kind=kLoop, calls=%fused_computation.21 | loop fusion | flops 3670016 | bytes 4195584 | tf_op jit(solution)/shard_map/reduce_sum | solution.py:115
  396.7 0.2 multiply_reduce_fusion.1
  397.0 1.4 fusion.41
  (62 shorter events, 0.9 us)
Async XLA Ops:
  6.5 1.0 copy-start.6
  6.5 9.3 %copy-start.12 = (s32[1,128,2]{1,2,0:T(2,128)S(1)}, s32[1,128,2]{1,2,0:T(2,128)}, u32[]{:S(2)}) copy-start(s32[1,128,2]{1,2,0:T(2,128)} %param.23) | copy-start | bytes 3076
  6.5 9.7 %copy-start.7 = (bf16[1,128,16,128]{3,2,1,0:T(8,128)(2,1)S(1)}, bf16[1,128,16,128]{3,2,1,0:T(8,128)(2,1)}, u32[]{:S(2)}) copy-start(bf16[1,128,16,128]{3,2,1,0:T(8,128)(2,1)} %param.14) | copy-start | bytes 1572868
  6.5 10.6 %copy-start.8 = (bf16[1,128,16,128]{3,2,1,0:T(8,128)(2,1)S(1)}, bf16[1,128,16,128]{3,2,1,0:T(8,128)(2,1)}, u32[]{:S(2)}) copy-start(bf16[1,128,16,128]{3,2,1,0:T(8,128)(2,1)} %param.15) | copy-start | bytes 1572868
  6.5 135.9 %all-gather.2.cloned.1.call-start = ((), (), s32[]{:S(2)}) async-start(), calls=%async_computation.6 | async-start | bytes 20971520 | tf_op jit(solution)/shard_map/all_gather | solution.py:72
  8.5 21.8 %all-to-all-start = ((bf16[1,128,16,128]{3,1,0,2:T(8,128)(2,1)}), bf16[1,128,16,128]{3,1,0,2:T(8,128)(2,1)S(1)}, u32[]{:S(2)}, u32[]{:S(2)}) async-start(bf16[1,128,16,128]{3,1,0,2:T(8,128)(2,1)} %copy.85), calls=%async_computation | async-start | bytes 1048576 | tf_op jit(solution)/shard_map/all_to_all | solution.py:62
  30.3 18.3 %all-to-all-start.1 = ((bf16[1,128,16,128]{3,1,0,2:T(8,128)(2,1)}), bf16[1,128,16,128]{3,1,0,2:T(8,128)(2,1)S(1)}, u32[]{:S(2)}, u32[]{:S(2)}) async-start(bf16[1,128,16,128]{3,1,0,2:T(8,128)(2,1)} %copy.87), calls=%async_computation.1 | async-start | bytes 1048576 | tf_op jit(solution)/shard_map/all_to_all | solution.py:63
  48.6 45.8 %all-to-all-start.2 = ((bf16[1,128,16,128]{3,1,0,2:T(8,128)(2,1)}), bf16[1,128,16,128]{3,1,0,2:T(8,128)(2,1)S(1)}, u32[]{:S(2)}, u32[]{:S(2)}) async-start(bf16[1,128,16,128]{3,1,0,2:T(8,128)(2,1)} %copy.91), calls=%async_computation.2 | async-start | bytes 1048576 | tf_op jit(solution)/shard_map/all_to_all | solution.py:64
  77.1 2.0 copy-start
  108.0 1.6 copy-start.4
  108.0 5.3 %copy-start.15 = (f32[2,512,1024]{2,1,0:T(8,128)S(1)}, f32[2,512,1024]{2,1,0:T(8,128)}, u32[]{:S(2)}) copy-start(f32[2,512,1024]{2,1,0:T(8,128)} %get-tuple-element.14) | copy-start | bytes 12582916
  109.6 3.7 copy-start.3
  122.0 20.1 %all-to-all-start.3 = ((bf16[1,1024,2,128]{3,2,0,1:T(2,128)(2,1)}), bf16[1,1024,2,128]{3,2,0,1:T(2,128)(2,1)S(1)}, u32[]{:S(2)}, u32[]{:S(2)}) async-start(bf16[1,1024,2,128]{3,2,0,1:T(2,128)(2,1)} %copy.96), calls=%async_computation.3 | async-start | bytes 1048576 | tf_op jit(solution)/shard_map/all_to_all | solution.py:67
  142.5 8.3 %copy-start.5 = (bf16[1,128,4096]{2,1,0:T(8,128)(2,1)S(1)}, bf16[1,128,4096]{2,1,0:T(8,128)(2,1)}, u32[]{:S(2)}) copy-start(bf16[1,128,4096]{2,1,0:T(8,128)(2,1)} %param.16) | copy-start | bytes 3145732
  142.5 8.3 %copy-start.9 = (f32[4096]{0:T(1024)S(1)}, f32[4096]{0:T(1024)}, u32[]{:S(2)}) copy-start(f32[4096]{0:T(1024)} %param.18) | copy-start | bytes 49156
  150.8 1.7 copy-start.10
  151.5 1.0 copy-start.1
  260.0 2.2 copy-start.14
  279.4 4.2 %copy-start.13 = (f32[1,128,2]{1,2,0:T(2,128)S(1)}, f32[1,128,2]{1,2,0:T(2,128)}, u32[]{:S(2)}) copy-start(f32[1,128,2]{1,2,0:T(2,128)} %param.24) | copy-start | bytes 3076
  279.4 98.1 %all-to-all-start.5 = ((bf16[12,32,4096]{2,0,1:T(8,128)(2,1)}), bf16[12,32,4096]{2,0,1:T(8,128)(2,1)}, u32[]{:S(2)}, u32[]{:S(2)}) async-start(bf16[12,32,4096]{2,0,1:T(8,128)(2,1)} %copy.108), calls=%async_computation.5 | async-start | bytes 8388608 | tf_op jit(solution)/shard_map/all_to_all | solution.py:106
  388.0 9.0 %copy-start.2 = (bf16[128,4096]{1,0:T(8,128)(2,1)S(1)}, bf16[128,4096]{1,0:T(8,128)(2,1)}, u32[]{:S(2)}) copy-start(bf16[128,4096]{1,0:T(8,128)(2,1)} %copy-done.1) | copy-start | bytes 3145732
  388.0 9.0 %copy-start.11 = (f32[4096]{0:T(1024)S(1)}, f32[4096]{0:T(1024)}, u32[]{:S(2)}) copy-start(f32[4096]{0:T(1024)} %param.25) | copy-start | bytes 49156
Sparse Core Ops, SparseCore 0:
  8.9 108.6 all-gather.1
where the time goes:
time: 412 us; the launch traced here: 406 us
  waiting for transfers between devices  132 us (32%)
  blocking collectives  97.3 us (24%)
  local copies, waits for them, and re-layouts  54.3 us (13%)
  other arithmetic  47.4 us (12%)
  matrix products  35.9 us (9%)
  starting transfers between devices  24.4 us (6%)
  between operations  14.3 us (3%)
    all_to_all x1, blocking collectives, local(): lax.all_to_all(outgoing, ('sp', 'dp'), split_axis=1, concat_axis=1, tiled...  97.3 us
    all_to_all x1, waiting for transfers between devices, local(): lax.all_to_all(result.reshape(slot_count, sources, width_now), ('sp', 'dp...  93.7 us
    another operation x6, other arithmetic  21.2 us
    all_to_all x1, waiting for transfers between devices, local(): lax.all_to_all(key_rows, 'sp', split_axis=2, concat_axis=1, tiled=True)  13.2 us
    all_to_all x1, waiting for transfers between devices, local(): lax.all_to_all(queries, 'sp', split_axis=2, concat_axis=1, tiled=True)  12.2 us
    all_to_all x1, waiting for transfers between devices, local(): lax.all_to_all(attended[None], 'sp', split_axis=1, concat_axis=2, tiled=T...  12.2 us
    another operation x3, local copies, waits for them, and re-layouts, attend(): suffix = lax.cumsum(log_keep, axis=2, reverse=True) - log_keep  11.2 us
    unnamed x37, local copies, waits for them, and re-layouts  10.5 us
  transfers between devices with their start and end apart: 6, of which 4 were waited for; matrix products, arithmetic and copies ran while one was open for 18% of the time, Pallas kernels for 0%

commit v1 on v0

v1 whole, which is shorter than its diff:
```python
import functools

import jax
import jax.numpy as jnp
from jax import lax
from jax.experimental import pallas as pl
from jax.experimental.pallas import tpu as pltpu
from jax.sharding import PartitionSpec as P

EPSILON = 1e-06
MESH = pl.DeviceIdType.MESH
VMEM_LIMIT = 56 * 1024 * 1024


def normed_token_rows(matrix, gain):
    return matrix * lax.rsqrt(jnp.mean(matrix * matrix, axis=-1, keepdims=True) + EPSILON) * gain


def peer_id(axes, sizes, flat):
    if len(axes) == 1:
        return {axes[0]: flat}
    return {axes[0]: lax.div(flat, sizes[1]), axes[1]: lax.rem(flat, sizes[1])}


def exchange_kernel(axes, sizes, n, count, *refs):
    ins, outs = refs[:count], refs[count : 2 * count]
    stages = refs[2 * count : 3 * count]
    send_sem, recv_sem, local_sem = refs[3 * count :]
    me = lax.axis_index(axes[0])
    if len(axes) == 2:
        me = me * sizes[1] + lax.axis_index(axes[1])

    barrier = pltpu.get_barrier_semaphore()

    def greet(k, carry):
        pl.semaphore_signal(
            barrier, inc=1, device_id=peer_id(axes, sizes, lax.rem(me + k, n)), device_id_type=MESH
        )
        return carry

    lax.fori_loop(1, n, greet, 0)
    loads = [
        pltpu.make_async_copy(ins[a].at[me], stages[a], local_sem.at[a]) for a in range(count)
    ]
    for load in loads:
        load.start()
    pl.semaphore_wait(barrier, n - 1)

    def copies(k):
        target = lax.rem(me + k, n)
        return [
            pltpu.make_async_remote_copy(
                src_ref=ins[a].at[target],
                dst_ref=outs[a].at[me],
                send_sem=send_sem.at[a, k],
                recv_sem=recv_sem.at[a, k],
                device_id=peer_id(axes, sizes, target),
                device_id_type=MESH,
            )
            for a in range(count)
        ]

    def push(i, carry):
        k = n // 2 + (1 - 2 * lax.rem(i, 2)) * lax.div(i + 1, 2)
        for copy in copies(k):
            copy.start()
        return carry

    lax.fori_loop(0, n - 1, push, 0)
    stores = [
        pltpu.make_async_copy(stages[a], outs[a].at[me], local_sem.at[a]) for a in range(count)
    ]
    for load in loads:
        load.wait()
    for store in stores:
        store.start()
    for store in stores:
        store.wait()

    def finish(k, carry):
        for copy in copies(k):
            copy.wait()
        return carry

    lax.fori_loop(1, n, finish, 0)


def exchange(arrays, axes, collective_id):
    sizes = [lax.axis_size(a) for a in axes]
    n = arrays[0].shape[0]
    count = len(arrays)
    moved = sum(a.size * 2 for a in arrays)
    return pl.pallas_call(
        functools.partial(exchange_kernel, axes, sizes, n, count),
        out_shape=[jax.ShapeDtypeStruct(a.shape, a.dtype) for a in arrays],
        in_specs=[pl.BlockSpec(memory_space=pl.ANY)] * count,
        out_specs=[pl.BlockSpec(memory_space=pl.ANY)] * count,
        scratch_shapes=[pltpu.VMEM(a.shape[1:], a.dtype) for a in arrays]
        + [
            pltpu.SemaphoreType.DMA((count, n)),
            pltpu.SemaphoreType.DMA((count, n)),
            pltpu.SemaphoreType.DMA((count,)),
        ],
        compiler_params=pltpu.CompilerParams(
            collective_id=collective_id, has_side_effects=True, vmem_limit_bytes=VMEM_LIMIT
        ),
        cost_estimate=pl.CostEstimate(flops=0, bytes_accessed=moved * 20, transcendentals=0),
    )(*arrays)


def attend_kernel(block, q_ref, k_ref, v_ref, out_ref):
    sources, _, rows, width = q_ref.shape
    length = sources * rows
    scale = width ** (-0.5)
    tri_row = lax.broadcasted_iota(jnp.int32, (block, block), 0)
    tri_col = lax.broadcasted_iota(jnp.int32, (block, block), 1)
    suffix_ones = (tri_row >= tri_col).astype(jnp.bfloat16)
    is_past = tri_col < tri_row
    per = block // rows

    def piece(ref, index):
        return ref[index * per : (index + 1) * per, 0].reshape(block, width)

    for q_block in range(length // block):
        query = piece(q_ref, q_block)
        total = jnp.zeros((block, width), jnp.float32)
        later = jnp.zeros((block, 1), jnp.float32)
        for k_block in range(q_block, -1, -1):
            scores = (
                lax.dot_general(
                    query,
                    piece(k_ref, k_block),
                    (((1,), (1,)), ((), ())),
                    preferred_element_type=jnp.float32,
                )
                * scale
            )
            soft = jnp.maximum(scores, 0.0) + jnp.log(1.0 + jnp.exp(-jnp.abs(scores)))
            if k_block == q_block:
                soft = jnp.where(is_past, soft, 0.0)
            high = soft.astype(jnp.bfloat16)
            low = (soft - high.astype(jnp.float32)).astype(jnp.bfloat16)
            suffix = jnp.dot(high, suffix_ones, preferred_element_type=jnp.float32) + jnp.dot(
                low, suffix_ones, preferred_element_type=jnp.float32
            )
            weights = jnp.exp(scores - suffix - later)
            if k_block == q_block:
                weights = jnp.where(is_past, weights, 0.0)
            total = total + jnp.dot(
                weights.astype(jnp.bfloat16),
                piece(v_ref, k_block),
                preferred_element_type=jnp.float32,
            )
            if k_block > 0:
                later = later + suffix[:, :1]
        out_ref[q_block * per : (q_block + 1) * per, 0] = total.astype(jnp.bfloat16).reshape(
            per, rows, width
        )


def attend(query, key, value):
    sources, heads, rows, width = query.shape
    block = rows * max(1, min(sources, 256 // rows))
    spec = pl.BlockSpec((sources, 1, rows, width), lambda h: (0, h, 0, 0))
    return pl.pallas_call(
        functools.partial(attend_kernel, block),
        grid=(heads,),
        out_shape=jax.ShapeDtypeStruct(query.shape, jnp.bfloat16),
        in_specs=[spec] * 3,
        out_specs=spec,
        compiler_params=pltpu.CompilerParams(vmem_limit_bytes=VMEM_LIMIT),
        cost_estimate=pl.CostEstimate(
            flops=6 * heads * (sources * rows) ** 2 * width, bytes_accessed=8 * query.size, transcendentals=0
        ),
    )(query, key, value)


def mix_kernel(steps, attn_ref, weight_ref, resid_ref, mixer_ref, expert_ref, pick_ref,
               stream_ref, *rest):
    sent_refs, projected = rest[:-1], rest[-1]
    step = pl.program_id(0)
    heads = attn_ref.shape[0]
    columns = weight_ref.shape[1]
    flat = jnp.concatenate([attn_ref[h] for h in range(heads)], axis=1)
    start = pl.multiple_of(step * columns, columns)
    projected[:, pl.ds(start, columns)] = jnp.dot(
        flat, weight_ref[...], preferred_element_type=jnp.float32
    )

    @pl.when(step == steps - 1)
    def _():
        stream = (
            resid_ref[...].astype(jnp.float32)
            + normed_token_rows(projected[...], mixer_ref[...])
        ).astype(jnp.bfloat16)
        stream_ref[...] = stream
        tokens = normed_token_rows(stream.astype(jnp.float32), expert_ref[...]).astype(jnp.bfloat16)
        row = 0
        for ref in sent_refs:
            many = ref.shape[0]
            ref[...] = jnp.dot(
                pick_ref[row : row + many], tokens, preferred_element_type=jnp.float32
            ).astype(jnp.bfloat16)
            row += many


def mix(attn, weight, residual, mixer_gain, expert_gain, pick, splits):
    heads, rows, width = attn.shape
    depth, features = weight.shape
    columns = min(1024, features)
    steps = features // columns
    whole = lambda shape: pl.BlockSpec(shape, lambda i: (0,) * len(shape))
    return pl.pallas_call(
        functools.partial(mix_kernel, steps),
        grid=(steps,),
        out_shape=[jax.ShapeDtypeStruct((many, features), jnp.bfloat16) for many in [rows] + splits],
        in_specs=[
            whole(attn.shape),
            pl.BlockSpec((depth, columns), lambda i: (0, i)),
            whole(residual.shape),
            whole((1, features)),
            whole((1, features)),
            whole(pick.shape),
        ],
        out_specs=[whole((many, features)) for many in [rows] + splits],
        scratch_shapes=[pltpu.VMEM((rows, features), jnp.float32)],
        compiler_params=pltpu.CompilerParams(vmem_limit_bytes=VMEM_LIMIT),
    )(attn, weight, residual, mixer_gain[None], expert_gain[None], pick)


def expert_kernel(count, *refs):
    ins, (gate_ref, up_ref, down_ref) = refs[:count], refs[count : count + 3]
    outs = refs[count + 3 :]
    for a in range(count):
        rows = ins[a][...]
        gate = jnp.dot(rows, gate_ref[...], preferred_element_type=jnp.float32)
        upward = jnp.dot(rows, up_ref[...], preferred_element_type=jnp.float32)
        hidden = (gate / (1.0 + jnp.exp(-gate)) * upward).astype(jnp.bfloat16)
        outs[a][...] = jnp.dot(
            hidden, down_ref[...], preferred_element_type=jnp.float32
        ).astype(jnp.bfloat16)


def serve(arrays, gate, up, down):
    return pl.pallas_call(
        functools.partial(expert_kernel, len(arrays)),
        out_shape=[jax.ShapeDtypeStruct(a.shape, a.dtype) for a in arrays],
        in_specs=[pl.BlockSpec(memory_space=pltpu.VMEM)] * (len(arrays) + 3),
        out_specs=[pl.BlockSpec(memory_space=pltpu.VMEM)] * len(arrays),
        compiler_params=pltpu.CompilerParams(vmem_limit_bytes=VMEM_LIMIT),
    )(*arrays, gate, up, down)


def combine_kernel(count, *refs):
    ins = refs[:count]
    high_ref, low_ref, stream_ref, gain_ref, out_ref = refs[count:]
    combined, row = 0.0, 0
    for ref in ins:
        many = ref.shape[0]
        for share in (high_ref, low_ref):
            combined = combined + jnp.dot(
                share[:, row : row + many], ref[...], preferred_element_type=jnp.float32
            )
        row += many
    out_ref[...] = (
        stream_ref[...].astype(jnp.float32) + normed_token_rows(combined, gain_ref[...])
    ).astype(jnp.bfloat16)


def combine(arrays, high, low, stream, gain):
    return pl.pallas_call(
        functools.partial(combine_kernel, len(arrays)),
        out_shape=jax.ShapeDtypeStruct(stream.shape, jnp.bfloat16),
        in_specs=[pl.BlockSpec(memory_space=pltpu.VMEM)] * (len(arrays) + 4),
        out_specs=pl.BlockSpec(memory_space=pltpu.VMEM),
        compiler_params=pltpu.CompilerParams(vmem_limit_bytes=VMEM_LIMIT),
    )(*arrays, high, low, stream, gain[None])


def local(
    queries,
    key_rows,
    values,
    residual,
    out_weight,
    mixer_gain,
    expert_gain,
    gate_weight,
    up_weight,
    expert_down_matrix,
    routes,
    route_weight,
    output_gain,
):
    full_weight = lax.all_gather(out_weight, "dp", axis=1, tiled=True)
    sp = lax.axis_size("sp")
    _, local_rows, heads, width = queries.shape
    features = residual.shape[2]

    def by_head(tensor):
        return jnp.transpose(tensor[0], (1, 0, 2)).reshape(sp, heads // sp, local_rows, width)

    head_parts = exchange([by_head(queries), by_head(key_rows), by_head(values)], ("sp",), 0)
    attended = attend(*head_parts)
    (token_parts,) = exchange([attended], ("sp",), 1)

    experts = sp * lax.axis_size("dp")
    top_count = routes.shape[2]
    capacity = max(2, 3 * local_rows // experts)
    picked = routes[0].reshape(local_rows * top_count)
    onehot = (
        picked[:, None] == lax.broadcasted_iota(jnp.int32, (picked.shape[0], experts), 1)
    ).astype(jnp.bfloat16)
    count = picked.shape[0]
    earlier = (
        lax.broadcasted_iota(jnp.int32, (count, count), 1)
        < lax.broadcasted_iota(jnp.int32, (count, count), 0)
    ).astype(jnp.bfloat16)
    before = jnp.dot(earlier, onehot, preferred_element_type=jnp.float32)
    rank = jnp.sum(before * onehot.astype(jnp.float32), axis=1).astype(jnp.int32)
    groups = [g for g in (capacity // 8 * 8, capacity % 8) if g]
    splits = [g * experts for g in groups]
    slot, first, base = jnp.full((count,), -1, jnp.int32), 0, 0
    for g in groups:
        inside = (rank >= first) & (rank < first + g)
        slot = jnp.where(inside, base + picked * g + rank - first, slot)
        first, base = first + g, base + g * experts
    slot = slot.reshape(local_rows, top_count)
    slot_ids = lax.broadcasted_iota(jnp.int32, (local_rows, base), 1)
    hits = [slot[:, k : k + 1] == slot_ids for k in range(top_count)]
    pick = functools.reduce(jnp.logical_or, hits).astype(jnp.bfloat16).T
    share = sum(jnp.where(hits[k], route_weight[0][:, k : k + 1], 0.0) for k in range(top_count))
    share_high = share.astype(jnp.bfloat16)
    share_low = (share - share_high.astype(jnp.float32)).astype(jnp.bfloat16)

    stream, *outgoing = mix(
        token_parts.reshape(heads, local_rows, width),
        full_weight,
        residual[0],
        mixer_gain,
        expert_gain,
        pick,
        splits,
    )

    def blocks(arrays):
        return [a.reshape(experts, g, features) for a, g in zip(arrays, groups)]

    def flat(arrays):
        return [a.reshape(-1, features) for a in arrays]

    arrived = exchange(blocks(outgoing), ("sp", "dp"), 2)
    results = serve(flat(arrived), gate_weight[0], up_weight[0], expert_down_matrix[0])
    returned = exchange(blocks(results), ("sp", "dp"), 3)
    output = combine(flat(returned), share_high, share_low, stream, output_gain)
    return output[None]


def solution(mesh):
    in_specs = (
        P("dp", "sp", None, None),
        P("dp", "sp", None, None),
        P("dp", "sp", None, None),
        P("dp", "sp", None),
        P(None, "dp"),
        P(),
        P(),
        P(("sp", "dp"), None, None),
        P(("sp", "dp"), None, None),
        P(("sp", "dp"), None, None),
        P("dp", "sp", None),
        P("dp", "sp", None),
        P(),
    )
    out_specs = P("dp", "sp", None)
    return jax.shard_map(local, mesh=mesh, in_specs=in_specs, out_specs=out_specs, check_vma=False)
```

time: 412 us -> 320 us (0.78)
  the two profiles are of different devices: /device:TPU:0 before, /device:TPU:16 now
where the time goes in v1:
time: 320 us
  Pallas kernels  250 us (78%)
  waiting for transfers between devices  42.1 us (13%)
  between operations  13.5 us (4%)
  local copies, waits for them, and re-layouts  12.3 us (4%)
    pallas_call x4, Pallas kernels, exchange(): pl.pallas_call(functools.partial(exchange_kernel, axes, sizes, n, count),...  213 us
    all_gather x1, waiting for transfers between devices, local(): full_weight = lax.all_gather(out_weight, 'dp', axis=1, tiled=True)  41.4 us
    pallas_call x1, Pallas kernels, serve(): pl.pallas_call(functools.partial(expert_kernel, len(arrays)), out_shape=[...  11.8 us
    pallas_call x1, Pallas kernels, mix(): pl.pallas_call(functools.partial(mix_kernel, steps), grid=(steps,), out_s...  11.5 us
    pallas_call x1, Pallas kernels, attend(): pl.pallas_call(functools.partial(attend_kernel, block), grid=(heads,), ou...  8.55 us
  transfers between devices with their start and end apart: 1, of which 1 were waited for; matrix products, arithmetic and copies ran while one was open for 2% of the time, Pallas kernels for 19%

profile of v1, /device:TPU:16, one launch (start us, length us, event | category | flops | bytes accessed | tf_op | source)
XLA Modules:
  0.0 319.8 jit_solution(13003632602239787866)
XLA Ops:
  6.5 0.0 copy-start
  6.5 0.0 copy-start.1
  6.5 0.0 copy-start.2
  6.5 0.0 all-gather.2.cloned.1.call-start
  6.5 0.7 all-gather.2.cloned.1.call-update
  7.3 0.3 copy-done
  7.6 0.9 copy.31
  8.5 0.0 copy-done.1
  8.5 0.9 copy.32
  9.5 0.0 copy-done.2
  9.5 0.9 copy.33
  10.4 0.0 copy-start.3
  10.4 0.0 copy-start.4
  10.4 38.9 %shard_map.127 = (bf16[8,2,128,128]{3,2,1,0:T(8,128)(2,1)}, bf16[8,2,128,128]{3,2,1,0:T(8,128)(2,1)}, bf16[8,2,128,128]{3,2,1,0:T(8,128)(2,1)}) custom-call(bf16[8,2,128,128]{3,2,1,0:T(8,128)(2,1)} %bitcast.49, bf16[8,2,128,128]{3,2,1,0:T(8,128)(2,1)} %bitcast.50, bf16[8,2,128,128]{3,2,1,0:T(8,128)(2,1)} %bitcast.51), custom_call_target="tpu_custom_call" | custom-call | bytes 31457280 | tf_op jit(solution)/shard_map/pallas_call | solution.py:93
  49.3 8.5 %shard_map.128.refs_0_ = bf16[8,2,128,128]{3,2,1,0:T(8,128)(2,1)} custom-call(bf16[8,2,128,128]{3,2,1,0:T(8,128)(2,1)} %get-tuple-element.17.q_ref, bf16[8,2,128,128]{3,2,1,0:T(8,128)(2,1)} %get-tuple-element.18.k_ref, bf16[8,2,128,128]{3,2,1,0:T(8,128)(2,1)} %get-tuple-element.19.v_ref), custom_call_target="tpu_custom_call" | custom-call | flops 1610612736 | bytes 2097152 | tf_op jit(solution)/shard_map/pallas_call | solution.py:165
  57.9 14.3 %shard_map.129 = bf16[8,2,128,128]{3,2,1,0:T(8,128)(2,1)} custom-call(bf16[8,2,128,128]{3,2,1,0:T(8,128)(2,1)} %shard_map.128.refs_0_), custom_call_target="tpu_custom_call" | custom-call | bytes 10485760 | tf_op jit(solution)/shard_map/pallas_call | solution.py:93
  72.2 0.0 copy-done.3
  72.2 0.1 copy.34
  72.4 0.1 eq.40
  72.5 0.2 fusion
  72.7 0.1 convert_element_type.30
  72.9 0.1 copy.35
  73.0 0.0 copy-done.4
  73.0 0.7 fusion.3.pick_ref
  73.6 0.8 subtract_convert_fusion
  74.5 41.4 %all-gather.2.cloned.1.call-done.weight_ref = bf16[2048,4096]{1,0:T(8,128)(2,1)} async-done(((bf16[2048,1024]{1,0:T(8,128)(2,1)}), bf16[2048,4096]{1,0:T(8,128)(2,1)}) %all-gather.2.cloned.1.call-update) | async-done | bytes 16777232 | tf_op jit(solution)/shard_map/all_gather | solution.py:295
  115.9 11.5 %shard_map.130 = (bf16[128,4096]{1,0:T(8,128)(2,1)}, bf16[256,4096]{1,0:T(8,128)(2,1)}, bf16[128,4096]{1,0:T(8,128)(2,1)}) custom-call(bf16[16,128,128]{2,1,0:T(8,128)(2,1)} %bitcast.48, bf16[2048,4096]{1,0:T(8,128)(2,1)} %all-gather.2.cloned.1.call-done.weight_ref, bf16[128,4096]{1,0:T(8,128)(2,1)} %bitcast.55, f32[1,4096]{1,0:T(1,128)} %bitcast.59, ...), custom_call_target="tpu_custom_call" | custom-call | tf_op jit(solution)/shard_map/pallas_call | solution.py:213
  127.4 2.2 reshape.52.refs_1_
  129.7 80.6 %shard_map.131 = (bf16[32,8,4096]{2,1,0:T(8,128)(2,1)}, bf16[32,4,4096]{2,1,0:T(4,128)(2,1)}) custom-call(bf16[32,8,4096]{2,1,0:T(8,128)(2,1)} %bitcast.52, bf16[32,4,4096]{2,1,0:T(4,128)(2,1)} %reshape.52.refs_1_), custom_call_target="tpu_custom_call" | custom-call | bytes 62914560 | tf_op jit(solution)/shard_map/pallas_call | solution.py:93
  210.2 2.1 reshape.54.refs_1_
  212.4 11.8 %shard_map.132 = (bf16[256,4096]{1,0:T(8,128)(2,1)}, bf16[128,4096]{1,0:T(8,128)(2,1)}) custom-call(bf16[256,4096]{1,0:T(8,128)(2,1)} %bitcast.47, bf16[128,4096]{1,0:T(8,128)(2,1)} %reshape.54.refs_1_, bf16[4096,512]{1,0:T(8,128)(2,1)} %bitcast.44, bf16[4096,512]{1,0:T(8,128)(2,1)} %bitcast.45, bf16[512,4096]{1,0:T(8,128)(2,1)} %bitcast.46), custom_call_target="tpu_custom_call" | custom-call | tf_op jit(solution)/shard_map/pallas_call | solution.py:245
  224.1 2.2 reshape.56.refs_1_
  226.4 79.4 %shard_map.133 = (bf16[32,8,4096]{2,1,0:T(8,128)(2,1)}, bf16[32,4,4096]{2,1,0:T(4,128)(2,1)}) custom-call(bf16[32,8,4096]{2,1,0:T(8,128)(2,1)} %bitcast.53, bf16[32,4,4096]{2,1,0:T(4,128)(2,1)} %reshape.56.refs_1_), custom_call_target="tpu_custom_call" | custom-call | bytes 62914560 | tf_op jit(solution)/shard_map/pallas_call | solution.py:93
  305.8 2.1 reshape.58.refs_1_
  307.9 5.1 %shard_map.134 = bf16[128,4096]{1,0:T(8,128)(2,1)} custom-call(bf16[256,4096]{1,0:T(8,128)(2,1)} %bitcast.54, bf16[128,4096]{1,0:T(8,128)(2,1)} %reshape.58.refs_1_, bf16[128,384]{1,0:T(8,128)(2,1)} %get-tuple-element.30.refs_2_, bf16[128,384]{1,0:T(8,128)(2,1)} %get-tuple-element.29.refs_3_, bf16[128,4096]{1,0:T(8,128)(2,1)} %get-tuple-element.28.refs_4_, ...), custom_call_target="tpu_custom_call" | custom-call | tf_op jit(solution)/shard_map/pallas_call | solution.py:271
  (4 shorter events, 0.0 us)
Async XLA Ops:
  6.5 1.0 copy-start
  6.5 2.0 copy-start.1
  6.5 2.9 copy-start.2
  6.5 109.4 %all-gather.2.cloned.1.call-start = ((), (), s32[]{:S(2)}) async-start(), calls=%async_computation | async-start | bytes 20971520 | tf_op jit(solution)/shard_map/all_gather | solution.py:295
  10.4 61.8 %copy-start.3 = (s32[1,128,2]{1,2,0:T(2,128)S(1)}, s32[1,128,2]{1,2,0:T(2,128)}, u32[]{:S(2)}) copy-start(s32[1,128,2]{1,2,0:T(2,128)} %param.23) | copy-start | bytes 3076
  10.4 62.6 %copy-start.4 = (f32[1,128,2]{1,2,0:T(2,128)S(1)}, f32[1,128,2]{1,2,0:T(2,128)}, u32[]{:S(2)}) copy-start(f32[1,128,2]{1,2,0:T(2,128)} %param.24) | copy-start | bytes 3076
Sparse Core Ops, SparseCore 0:
  8.9 106.9 all-gather.1

commit v2 on v1

--- a/solution.py
+++ b/solution.py
@@ -175,57 +175,52 @@
     )(query, key, value)
 
 
-def mix_kernel(steps, attn_ref, weight_ref, resid_ref, mixer_ref, expert_ref, pick_ref,
-               stream_ref, *rest):
-    sent_refs, projected = rest[:-1], rest[-1]
-    step = pl.program_id(0)
-    heads = attn_ref.shape[0]
-    columns = weight_ref.shape[1]
-    flat = jnp.concatenate([attn_ref[h] for h in range(heads)], axis=1)
-    start = pl.multiple_of(step * columns, columns)
-    projected[:, pl.ds(start, columns)] = jnp.dot(
-        flat, weight_ref[...], preferred_element_type=jnp.float32
+def project_kernel(attn_ref, weight_ref, out_ref):
+    for part in range(attn_ref.shape[0]):
+        flat = jnp.concatenate([attn_ref[part, h] for h in range(attn_ref.shape[1])], axis=1)
+        out_ref[part] = jnp.dot(
+            flat, weight_ref[...], preferred_element_type=jnp.float32
+        ).astype(jnp.bfloat16)
+
+
+def project(attn, weight):
+    parts, _, rows, _ = attn.shape
+    return pl.pallas_call(
+        project_kernel,
+        out_shape=jax.ShapeDtypeStruct((parts, rows, weight.shape[1]), jnp.bfloat16),
+        in_specs=[pl.BlockSpec(memory_space=pltpu.VMEM)] * 2,
+        out_specs=pl.BlockSpec(memory_space=pltpu.VMEM),
+        compiler_params=pltpu.CompilerParams(vmem_limit_bytes=VMEM_LIMIT),
+    )(attn, weight)
+
+
+def mix_kernel(parts_ref, resid_ref, mixer_ref, expert_ref, pick_ref, stream_ref, *sent_refs):
+    projected = jnp.concatenate(
+        [parts_ref[part].astype(jnp.float32) for part in range(parts_ref.shape[0])], axis=1
     )
-
-    @pl.when(step == steps - 1)
-    def _():
-        stream = (
-            resid_ref[...].astype(jnp.float32)
-            + normed_token_rows(projected[...], mixer_ref[...])
+    stream = (
+        resid_ref[...].astype(jnp.float32) + normed_token_rows(projected, mixer_ref[...])
+    ).astype(jnp.bfloat16)
+    stream_ref[...] = stream
+    tokens = normed_token_rows(stream.astype(jnp.float32), expert_ref[...]).astype(jnp.bfloat16)
+    row = 0
+    for ref in sent_refs:
+        many = ref.shape[0]
+        ref[...] = jnp.dot(
+            pick_ref[row : row + many], tokens, preferred_element_type=jnp.float32
         ).astype(jnp.bfloat16)
-        stream_ref[...] = stream
-        tokens = normed_token_rows(stream.astype(jnp.float32), expert_ref[...]).astype(jnp.bfloat16)
-        row = 0
-        for ref in sent_refs:
-            many = ref.shape[0]
-            ref[...] = jnp.dot(
-                pick_ref[row : row + many], tokens, preferred_element_type=jnp.float32
-            ).astype(jnp.bfloat16)
-            row += many
-
-
-def mix(attn, weight, residual, mixer_gain, expert_gain, pick, splits):
-    heads, rows, width = attn.shape
-    depth, features = weight.shape
-    columns = min(1024, features)
-    steps = features // columns
-    whole = lambda shape: pl.BlockSpec(shape, lambda i: (0,) * len(shape))
-    return pl.pallas_call(
-        functools.partial(mix_kernel, steps),
-        grid=(steps,),
+        row += many
+
+
+def mix(parts, residual, mixer_gain, expert_gain, pick, splits):
+    rows, features = residual.shape
+    return pl.pallas_call(
+        mix_kernel,
         out_shape=[jax.ShapeDtypeStruct((many, features), jnp.bfloat16) for many in [rows] + splits],
-        in_specs=[
-            whole(attn.shape),
-            pl.BlockSpec((depth, columns), lambda i: (0, i)),
-            whole(residual.shape),
-            whole((1, features)),
-            whole((1, features)),
-            whole(pick.shape),
-        ],
-        out_specs=[whole((many, features)) for many in [rows] + splits],
-        scratch_shapes=[pltpu.VMEM((rows, features), jnp.float32)],
-        compiler_params=pltpu.CompilerParams(vmem_limit_bytes=VMEM_LIMIT),
-    )(attn, weight, residual, mixer_gain[None], expert_gain[None], pick)
+        in_specs=[pl.BlockSpec(memory_space=pltpu.VMEM)] * 5,
+        out_specs=[pl.BlockSpec(memory_space=pltpu.VMEM)] * (1 + len(splits)),
+        compiler_params=pltpu.CompilerParams(vmem_limit_bytes=VMEM_LIMIT),
+    )(parts, residual, mixer_gain[None], expert_gain[None], pick)
 
 
 def expert_kernel(count, *refs):
@@ -292,7 +287,6 @@
     route_weight,
     output_gain,
 ):
-    full_weight = lax.all_gather(out_weight, "dp", axis=1, tiled=True)
     sp = lax.axis_size("sp")
     _, local_rows, heads, width = queries.shape
     features = residual.shape[2]
@@ -304,7 +298,12 @@
     attended = attend(*head_parts)
     (token_parts,) = exchange([attended], ("sp",), 1)
 
-    experts = sp * lax.axis_size("dp")
+    dp = lax.axis_size("dp")
+    token_heads = token_parts.reshape(heads, local_rows, width)
+    (group_heads,) = exchange([jnp.broadcast_to(token_heads[None], (dp,) + token_heads.shape)], ("dp",), 4)
+    (projected_parts,) = exchange([project(group_heads, out_weight)], ("dp",), 5)
+
+    experts = sp * dp
     top_count = routes.shape[2]
     capacity = max(2, 3 * local_rows // experts)
     picked = routes[0].reshape(local_rows * top_count)
@@ -334,8 +333,7 @@
     share_low = (share - share_high.astype(jnp.float32)).astype(jnp.bfloat16)
 
     stream, *outgoing = mix(
-        token_parts.reshape(heads, local_rows, width),
-        full_weight,
+        projected_parts,
         residual[0],
         mixer_gain,
         expert_gain,

time: 320 us -> 307 us (0.959)
  waiting for transfers between devices: 42.1 us -> 0 us
  Pallas kernels: 250 us -> 288 us
  between operations: 13.5 us -> 0.1 us
  local copies, waits for them, and re-layouts: 12.3 us -> 17.1 us
    all_gather x1 -> x0, waiting for transfers between devices: 41.4 us -> none  [local(): full_weight = lax.all_gather(out_weight, 'dp', axis=1, tiled=True)]
    pallas_call x4 -> x6, Pallas kernels: 213 us -> 252 us  [exchange(): pl.pallas_call(functools.partial(exchange_kernel, axes, sizes, n, count),...]
    pallas_call x1 -> x2, Pallas kernels: 11.5 us -> 10.8 us  [the longest x1 6.14 us: project(): pl.pallas_call(project_kernel, out_shape=jax.ShapeDtypeStruct((parts, row...]
  transfers between devices with their start and end apart: 1 -> 0, of which waited for: 1 -> 0; matrix products, arithmetic and copies ran while one was open for 2% -> 0% of each run, Pallas kernels for 19% -> 0%
where the time goes in v2:
time: 307 us
  Pallas kernels  288 us (94%)
  local copies, waits for them, and re-layouts  17.1 us (6%)
    pallas_call x6, Pallas kernels, exchange(): pl.pallas_call(functools.partial(exchange_kernel, axes, sizes, n, count),...  252 us
    pallas_call x1, Pallas kernels, serve(): pl.pallas_call(functools.partial(expert_kernel, len(arrays)), out_shape=[...  11.8 us
    pallas_call x1, Pallas kernels, attend(): pl.pallas_call(functools.partial(attend_kernel, block), grid=(heads,), ou...  8.55 us
    pallas_call x1, Pallas kernels, project(): pl.pallas_call(project_kernel, out_shape=jax.ShapeDtypeStruct((parts, row...  6.14 us

profile of v2, /device:TPU:16, one launch (start us, length us, event | category | flops | bytes accessed | tf_op | source)
XLA Modules:
  0.0 306.9 jit_solution(3955832125532476193)
XLA Ops:
  0.0 0.0 copy-start
  0.0 2.0 copy.31
  2.0 2.0 copy.32
  4.0 0.0 copy-done
  4.0 0.9 copy.33
  5.0 38.9 %shard_map.127 = (bf16[8,2,128,128]{3,2,1,0:T(8,128)(2,1)}, bf16[8,2,128,128]{3,2,1,0:T(8,128)(2,1)}, bf16[8,2,128,128]{3,2,1,0:T(8,128)(2,1)}) custom-call(bf16[8,2,128,128]{3,2,1,0:T(8,128)(2,1)} %bitcast.48, bf16[8,2,128,128]{3,2,1,0:T(8,128)(2,1)} %bitcast.49, bf16[8,2,128,128]{3,2,1,0:T(8,128)(2,1)} %bitcast.50), custom_call_target="tpu_custom_call" | custom-call | bytes 31457280 | tf_op jit(solution)/shard_map/pallas_call | solution.py:93
  43.9 8.6 %shard_map.128.refs_0_ = bf16[8,2,128,128]{3,2,1,0:T(8,128)(2,1)} custom-call(bf16[8,2,128,128]{3,2,1,0:T(8,128)(2,1)} %get-tuple-element.17.q_ref, bf16[8,2,128,128]{3,2,1,0:T(8,128)(2,1)} %get-tuple-element.18.k_ref, bf16[8,2,128,128]{3,2,1,0:T(8,128)(2,1)} %get-tuple-element.19.v_ref), custom_call_target="tpu_custom_call" | custom-call | flops 1610612736 | bytes 2097152 | tf_op jit(solution)/shard_map/pallas_call | solution.py:165
  52.5 14.3 %shard_map.129 = bf16[8,2,128,128]{3,2,1,0:T(8,128)(2,1)} custom-call(bf16[8,2,128,128]{3,2,1,0:T(8,128)(2,1)} %shard_map.128.refs_0_), custom_call_target="tpu_custom_call" | custom-call | bytes 10485760 | tf_op jit(solution)/shard_map/pallas_call | solution.py:93
  66.8 2.9 broadcast_in_dim.45.refs_0_
  69.7 25.3 %shard_map.130.attn_ref = bf16[4,16,128,128]{3,2,1,0:T(8,128)(2,1)} custom-call(bf16[4,16,128,128]{3,2,1,0:T(8,128)(2,1)} %broadcast_in_dim.45.refs_0_), custom_call_target="tpu_custom_call" | custom-call | bytes 41943040 | tf_op jit(solution)/shard_map/pallas_call | solution.py:93
  95.0 6.1 %shard_map.131.refs_0_ = bf16[4,128,1024]{2,1,0:T(8,128)(2,1)} custom-call(bf16[4,16,128,128]{3,2,1,0:T(8,128)(2,1)} %shard_map.130.attn_ref, bf16[2048,1024]{1,0:T(8,128)(2,1)} %weight_ref.1), custom_call_target="tpu_custom_call" | custom-call | tf_op jit(solution)/shard_map/pallas_call | solution.py:188
  101.1 0.0 copy-start.1
  101.1 14.0 %shard_map.132.parts_ref = bf16[4,128,1024]{2,1,0:T(8,128)(2,1)} custom-call(bf16[4,128,1024]{2,1,0:T(8,128)(2,1)} %shard_map.131.refs_0_), custom_call_target="tpu_custom_call" | custom-call | bytes 20971520 | tf_op jit(solution)/shard_map/pallas_call | solution.py:93
  115.2 0.0 copy-done.1
  115.2 0.1 copy.34
  115.3 0.1 eq.40
  115.5 0.2 fusion
  115.7 0.1 convert_element_type.30
  115.8 0.1 copy.35
  115.9 0.7 fusion.3.pick_ref
  116.6 4.6 %shard_map.133 = (bf16[128,4096]{1,0:T(8,128)(2,1)}, bf16[256,4096]{1,0:T(8,128)(2,1)}, bf16[128,4096]{1,0:T(8,128)(2,1)}) custom-call(bf16[4,128,1024]{2,1,0:T(8,128)(2,1)} %shard_map.132.parts_ref, bf16[128,4096]{1,0:T(8,128)(2,1)} %bitcast.55, f32[1,4096]{1,0:T(1,128)} %bitcast.59, f32[1,4096]{1,0:T(1,128)} %bitcast.60, bf16[384,128]{1,0:T(8,128)(2,1)} %fusion.3.pick_ref), custom_call_target="tpu_custom_call" | custom-call | tf_op jit(solution)/shard_map/pallas_call | solution.py:217
  121.2 2.2 reshape.49.refs_1_
  123.5 79.8 %shard_map.134 = (bf16[32,8,4096]{2,1,0:T(8,128)(2,1)}, bf16[32,4,4096]{2,1,0:T(4,128)(2,1)}) custom-call(bf16[32,8,4096]{2,1,0:T(8,128)(2,1)} %bitcast.52, bf16[32,4,4096]{2,1,0:T(4,128)(2,1)} %reshape.49.refs_1_), custom_call_target="tpu_custom_call" | custom-call | bytes 62914560 | tf_op jit(solution)/shard_map/pallas_call | solution.py:93
  203.2 2.1 reshape.51.refs_1_
  205.4 11.8 %shard_map.135 = (bf16[256,4096]{1,0:T(8,128)(2,1)}, bf16[128,4096]{1,0:T(8,128)(2,1)}) custom-call(bf16[256,4096]{1,0:T(8,128)(2,1)} %bitcast.47, bf16[128,4096]{1,0:T(8,128)(2,1)} %reshape.51.refs_1_, bf16[4096,512]{1,0:T(8,128)(2,1)} %bitcast.44, bf16[4096,512]{1,0:T(8,128)(2,1)} %bitcast.45, bf16[512,4096]{1,0:T(8,128)(2,1)} %bitcast.46), custom_call_target="tpu_custom_call" | custom-call | tf_op jit(solution)/shard_map/pallas_call | solution.py:240
  217.1 2.2 reshape.53.refs_1_
  219.4 0.0 copy-start.2
  219.4 79.4 %shard_map.136 = (bf16[32,8,4096]{2,1,0:T(8,128)(2,1)}, bf16[32,4,4096]{2,1,0:T(4,128)(2,1)}) custom-call(bf16[32,8,4096]{2,1,0:T(8,128)(2,1)} %bitcast.53, bf16[32,4,4096]{2,1,0:T(4,128)(2,1)} %reshape.53.refs_1_), custom_call_target="tpu_custom_call" | custom-call | bytes 62914560 | tf_op jit(solution)/shard_map/pallas_call | solution.py:93
  298.8 2.2 reshape.55.refs_1_
  301.0 0.0 copy-done.2
  301.0 0.8 subtract_convert_fusion
  301.8 5.1 %shard_map.137 = bf16[128,4096]{1,0:T(8,128)(2,1)} custom-call(bf16[256,4096]{1,0:T(8,128)(2,1)} %bitcast.54, bf16[128,4096]{1,0:T(8,128)(2,1)} %reshape.55.refs_1_, bf16[128,384]{1,0:T(8,128)(2,1)} %get-tuple-element.30.refs_2_, bf16[128,384]{1,0:T(8,128)(2,1)} %get-tuple-element.29.refs_3_, bf16[128,4096]{1,0:T(8,128)(2,1)} %get-tuple-element.28.refs_4_, ...), custom_call_target="tpu_custom_call" | custom-call | tf_op jit(solution)/shard_map/pallas_call | solution.py:266
  (4 shorter events, 0.0 us)
Async XLA Ops:
  0.0 4.0 %copy-start = (bf16[1,128,16,128]{3,2,1,0:T(8,128)(2,1)S(1)}, bf16[1,128,16,128]{3,2,1,0:T(8,128)(2,1)}, u32[]{:S(2)}) copy-start(bf16[1,128,16,128]{3,2,1,0:T(8,128)(2,1)} %param.15) | copy-start | bytes 1572868
  101.1 14.1 %copy-start.1 = (s32[1,128,2]{1,2,0:T(2,128)S(1)}, s32[1,128,2]{1,2,0:T(2,128)}, u32[]{:S(2)}) copy-start(s32[1,128,2]{1,2,0:T(2,128)} %param.23) | copy-start | bytes 3076
  219.4 81.6 %copy-start.2 = (f32[1,128,2]{1,2,0:T(2,128)S(1)}, f32[1,128,2]{1,2,0:T(2,128)}, u32[]{:S(2)}) copy-start(f32[1,128,2]{1,2,0:T(2,128)} %param.24) | copy-start | bytes 3076
